TPU v7x, 32 devices: a whole 2x2x4 slice. The times are simulated.
32 devices in a mesh: sp: 8 (over z, y), tp: 4 (over x, core).
Axes of the slice: x: 2, y: 2, z: 4, core: 2. Of those that a mesh axis runs over, the one named last changes fastest.
Arguments:
- residual: bfloat16 [4096, 2048], P(('sp', 'tp')), may hold values from -6 to 6
- query_proj: bfloat16 [4096, 2048], P('sp', 'tp'), may hold values from -12 to 12
- key_proj: bfloat16 [4096, 512], P('sp', 'tp'), may hold values from -12 to 12
- value_proj: bfloat16 [4096, 512], P('sp', 'tp'), may hold values from -6 to 6
- query_gain: float32 [128], replicated, may hold values from 0.4 to 4.5
- key_gain: float32 [128], replicated, may hold values from 0.4 to 4.5
- document_ids: int32 [4096], P('sp'), may hold values from 0 to 3, never falling along the last dimension, each value on 1 to 1537 neighbouring positions
- output_weight: bfloat16 [2048, 2048], replicated, may hold values from -0.125 to 0.125
- norm_gain: float32 [2048], replicated, may hold values from 0.1 to 1.9
- expert_ids: int32 [4096, 2], P(('sp', 'tp')), may hold values from 0 to 31, all different within a row; in each aligned block of 128 rows (0 to 127, 128 to 255, ...) at most 16 rows name the same one
- route_weights: float32 [4096, 2], P(('sp', 'tp')), may hold values from 0.2 to 1
- gate_weight: bfloat16 [32, 2048, 512], P(('sp', 'tp')), may hold values from -0.125 to 0.125
- up_weight: bfloat16 [32, 2048, 512], P(('sp', 'tp')), may hold values from -0.125 to 0.125
- down_weight: bfloat16 [32, 512, 2048], P(('sp', 'tp')), may hold values from -0.25 to 0.25
Outputs:
- updated: bfloat16 [4096, 2048], P(('sp', 'tp'))
Inputs may be any that keep to these rules, and one draw needn't show every extreme that they name: `document_ids`: document numbers never fall along the positions; each document has at most 1537 positions, and one has exactly 1537. `expert_ids`: each row names 2 different experts; within the rows of one device no expert is named more than 16 times, and in some device's rows an expert is named exactly 16 times.
All inputs are finite; a program needn't handle non-finite values.
Results may differ from a plain program's by a relative error of at most 0.017.
Values may be sent and summed in bfloat16 or wider, within the bound.
A program may use at most 128 MiB of HBM per device.

v0:
```python
import jax
import jax.numpy as jnp
from jax import lax
from jax.sharding import PartitionSpec as P

HEAD = 128
GRID_W = 64
REACH = 3


norm_eps = 1e-06
rope_base = 10000.0
masked_low = -1e30


def from_behind(block, axis, distance):
    devices = range(lax.axis_size(axis))
    route = [(i - distance, i) for i in devices if i - distance in devices]
    return lax.ppermute(block, axis, route)


def rotary_tables(first_row, length):
    freq_count = HEAD // 4
    inverse = 1.0 / rope_base ** (jnp.arange(freq_count, dtype=jnp.float32) / freq_count)
    position = first_row + jnp.arange(length, dtype=jnp.int32)
    grid_row = (position // GRID_W).astype(jnp.float32)
    grid_col = (position % GRID_W).astype(jnp.float32)
    angles = jnp.concatenate(
        [grid_row[:, None] * inverse[None, :], grid_col[:, None] * inverse[None, :]], axis=1
    )
    return (jnp.cos(angles), jnp.sin(angles))


def norm_rotate(projected, gains, cosine, sine_table):
    length = projected.shape[0]
    values_wide = projected.astype(jnp.float32).reshape(length, -1, HEAD)
    scaled = (
        values_wide
        * lax.rsqrt(jnp.mean(values_wide * values_wide, axis=-1, keepdims=True) + norm_eps)
        * gains
    )
    half_size = HEAD // 2
    first_half = scaled[..., :half_size]
    second_half = scaled[..., half_size:]
    cosine_rows = cosine[:, None, :]
    sine_rows = sine_table[:, None, :]
    turned = jnp.concatenate(
        [
            first_half * cosine_rows - second_half * sine_rows,
            first_half * sine_rows + second_half * cosine_rows,
        ],
        axis=-1,
    )
    return turned.reshape(length, -1).astype(jnp.bfloat16)


def on_device(
    residual,
    query_proj,
    key_proj,
    value_proj,
    query_gain,
    key_gain,
    document_ids,
    output_weight,
    norm_gain,
    expert_ids,
    route_weights,
    gate_weight,
    up_weight,
    down_weight,
):
    rows_here = query_proj.shape[0]
    cosine, sine_table = rotary_tables(lax.axis_index("sp") * rows_here, rows_here)
    query_norm = norm_rotate(query_proj, query_gain, cosine, sine_table)
    key_norm = norm_rotate(key_proj, key_gain, cosine, sine_table)
    key_heads = key_proj.shape[1] // HEAD
    groups = query_proj.shape[1] // key_proj.shape[1]
    query_grid = query_norm.reshape(rows_here, key_heads, groups, HEAD)
    local_doc = document_ids + 1
    start_carry = (
        jnp.full((key_heads, groups, rows_here), masked_low, jnp.float32),
        jnp.zeros((key_heads, groups, rows_here), jnp.float32),
        jnp.zeros((key_heads, groups, rows_here, HEAD), jnp.float32),
    )
    key_list = [key_norm]
    value_list = [value_proj]
    doc_list = [local_doc]
    for distance in range(1, REACH + 1):
        for direction in (1, -1):
            moved = from_behind((key_norm, value_proj, local_doc), "sp", direction * distance)
            key_list.append(moved[0])
            value_list.append(moved[1])
            doc_list.append(moved[2])
    key_part = jnp.concatenate(key_list, axis=0)
    value_part = jnp.concatenate(value_list, axis=0)
    doc_part = jnp.concatenate(doc_list, axis=0)
    part_rows = key_part.shape[0]

    def one_block(turn_index, inner):
        running_max, denominator, weighted = inner
        first_row = turn_index * rows_here
        key_block = lax.dynamic_slice_in_dim(key_part, first_row, rows_here, 0).reshape(
            rows_here, key_heads, HEAD
        )
        value_block = lax.dynamic_slice_in_dim(value_part, first_row, rows_here, 0).reshape(
            rows_here, key_heads, HEAD
        )
        doc_block = lax.dynamic_slice_in_dim(doc_part, first_row, rows_here, 0)
        scores = jnp.einsum(
            "qhgd,khd->hgqk", query_grid, key_block, preferred_element_type=jnp.float32
        ) * HEAD ** (-0.5)
        same_doc = (local_doc[:, None] == doc_block[None, :])[None, None]
        scores = jnp.where(same_doc, scores, masked_low)
        new_max = jnp.maximum(running_max, jnp.max(scores, axis=-1))
        weights = jnp.where(same_doc, jnp.exp(scores - new_max[..., None]), 0.0)
        rescale = jnp.exp(running_max - new_max)
        denominator = denominator * rescale + jnp.sum(weights, axis=-1)
        weighted = weighted * rescale[..., None] + jnp.einsum(
            "hgqk,khd->hgqd",
            weights.astype(jnp.bfloat16),
            value_block,
            preferred_element_type=jnp.float32,
        )
        return (new_max, denominator, weighted)

    final_carry = lax.fori_loop(0, part_rows // rows_here, one_block, start_carry)
    attn = jnp.transpose(final_carry[2] / final_carry[1][..., None], (2, 0, 1, 3))
    attn = attn.reshape(rows_here, key_heads * groups * HEAD).astype(jnp.bfloat16)
    token_rows = residual.shape[0]
    all_heads = lax.all_to_all(attn, "tp", split_axis=0, concat_axis=1, tiled=True)
    projected = jnp.dot(all_heads, output_weight, preferred_element_type=jnp.float32)
    hidden = (residual.astype(jnp.float32) + projected).astype(jnp.bfloat16)
    hidden_wide = hidden.astype(jnp.float32)
    normed = (
        hidden_wide
        * lax.rsqrt(jnp.mean(hidden_wide * hidden_wide, axis=-1, keepdims=True) + norm_eps)
        * norm_gain
    ).astype(jnp.bfloat16)
    top_count = expert_ids.shape[1]
    experts_all = lax.axis_size("sp") * lax.axis_size("tp")
    capacity = max(2, 2 * token_rows * top_count // experts_all)
    flat_ids = expert_ids.reshape(-1)
    onehot = (flat_ids[:, None] == jnp.arange(experts_all, dtype=jnp.int32)[None, :]).astype(
        jnp.int32
    )
    arrival = jnp.sum(jnp.cumsum(onehot, axis=0) * onehot, axis=1) - 1
    slot_index = flat_ids * capacity + arrival
    slot_grid = slot_index.reshape(token_rows, top_count)
    placing = jnp.sum(
        (
            jnp.arange(experts_all * capacity, dtype=jnp.int32)[:, None, None] == slot_grid[None]
        ).astype(jnp.float32),
        axis=2,
    ).astype(jnp.bfloat16)
    outgoing = jnp.dot(placing, normed, preferred_element_type=jnp.float32).astype(jnp.bfloat16)
    outgoing = outgoing.reshape(experts_all, capacity, normed.shape[1])
    arrived = lax.all_to_all(outgoing, ("sp", "tp"), split_axis=0, concat_axis=0, tiled=True)
    sources, slots, width = arrived.shape
    flat_rows = arrived.reshape(sources * slots, width)
    gate_part = jnp.dot(flat_rows, gate_weight[0], preferred_element_type=jnp.float32)
    up_part = jnp.dot(flat_rows, up_weight[0], preferred_element_type=jnp.float32)
    activity = (jax.nn.silu(gate_part) * up_part).astype(jnp.bfloat16)
    expert_out = jnp.dot(activity, down_weight[0], preferred_element_type=jnp.float32).astype(
        jnp.bfloat16
    )
    returned = lax.all_to_all(
        expert_out.reshape(sources, slots, width),
        ("sp", "tp"),
        split_axis=0,
        concat_axis=0,
        tiled=True,
    )
    fetched = returned.reshape(experts_all * capacity, -1)[slot_index]
    fetched = fetched.reshape(token_rows, top_count, -1).astype(jnp.float32)
    combined = jnp.sum(fetched * route_weights[..., None], axis=1)
    return (hidden_wide + combined).astype(jnp.bfloat16)


def solution(mesh):
    in_specs = (
        P(("sp", "tp"), None),
        P("sp", "tp"),
        P("sp", "tp"),
        P("sp", "tp"),
        P(),
        P(),
        P("sp"),
        P(),
        P(),
        P(("sp", "tp"), None),
        P(("sp", "tp"), None),
        P(("sp", "tp"), None, None),
        P(("sp", "tp"), None, None),
        P(("sp", "tp"), None, None),
    )
    out_specs = P(("sp", "tp"), None)
    return jax.shard_map(
        on_device, mesh=mesh, in_specs=in_specs, out_specs=out_specs, check_vma=False
    )
```

profile of v0, /device:TPU:0, one launch (start us, length us, event | category | flops | bytes accessed | tf_op | source)
XLA Modules:
  0.0 321.2 jit_solution(11046267321472765126)
XLA Ops:
  2.6 5.6 %collective-permute-start.6 = (bf16[512,128]{0,1:T(8,128)(2,1)S(1)}, bf16[512,128]{0,1:T(8,128)(2,1)}, u32[]{:S(2)}, u32[]{:S(2)}) collective-permute-start(bf16[512,128]{0,1:T(8,128)(2,1)S(1)} %maximum_bitcast_fusion), channel_id=1, source_target_pairs={{0,4},{4,8},{8,12},{12,16},{16,20},{20,24},{24,28},{1,5},{5,9},{9,... | collective-permute-start | bytes 393224 | tf_op jit(solution)/shard_map/ppermute | solution.py:19
  9.5 5.5 %collective-permute-start.8 = (bf16[512,128]{0,1:T(8,128)(2,1)S(1)}, bf16[512,128]{0,1:T(8,128)(2,1)}, u32[]{:S(2)}, u32[]{:S(2)}) collective-permute-start(bf16[512,128]{0,1:T(8,128)(2,1)S(1)} %maximum_bitcast_fusion), channel_id=1, source_target_pairs={{0,8},{4,12},{8,16},{12,20},{16,24},{20,28},{1,9},{5,13},{9,17},{1... | collective-permute-start | bytes 393224 | tf_op jit(solution)/shard_map/ppermute | solution.py:19
  17.0 2.5 collective-permute-start
  22.6 1.6 constant_dynamic-update-slice_fusion.14
  26.3 1.3 collective-permute-start.1
  27.6 5.6 %collective-permute-done.1 = s32[512]{0:T(512)S(1)} collective-permute-done((s32[512]{0:T(512)S(1)}, s32[512]{0:T(512)S(1)}, u32[]{:S(2)}, u32[]{:S(2)}) %collective-permute-start.1) | collective-permute-done | bytes 2080 | tf_op jit(solution)/shard_map/ppermute | solution.py:19
  33.3 3.1 collective-permute-start.2
  39.0 4.4 %collective-permute-done.3 = s32[512]{0:T(512)S(1)} collective-permute-done((s32[512]{0:T(512)S(1)}, s32[512]{0:T(512)S(1)}, u32[]{:S(2)}, u32[]{:S(2)}) %collective-permute-start.3) | collective-permute-done | bytes 2080 | tf_op jit(solution)/shard_map/ppermute | solution.py:19
  43.4 6.2 %collective-permute-start.4 = (s32[512]{0:T(512)S(1)}, s32[512]{0:T(512)S(1)}, u32[]{:S(2)}, u32[]{:S(2)}) collective-permute-start(s32[512]{0:T(512)S(1)} %get-tuple-element.328), channel_id=1, source_target_pairs={{0,12},{4,16},{8,20},{12,24},{16,28},{1,13},{5,17},{9,21},{13,25},... | collective-permute-start | bytes 6152 | tf_op jit(solution)/shard_map/ppermute | solution.py:19
  52.2 5.3 %collective-permute-done.5 = s32[512]{0:T(512)S(1)} collective-permute-done((s32[512]{0:T(512)S(1)}, s32[512]{0:T(512)S(1)}, u32[]{:S(2)}, u32[]{:S(2)}) %collective-permute-start.5) | collective-permute-done | bytes 2080 | tf_op jit(solution)/shard_map/ppermute | solution.py:19
  57.5 5.7 %collective-permute-start.10 = (bf16[512,128]{0,1:T(8,128)(2,1)S(1)}, bf16[512,128]{0,1:T(8,128)(2,1)S(1)}, u32[]{:S(2)}, u32[]{:S(2)}) collective-permute-start(bf16[512,128]{0,1:T(8,128)(2,1)S(1)} %maximum_bitcast_fusion), channel_id=1, source_target_pairs={{0,12},{4,16},{8,20},{12,24},{16,28},{1,13},{5,17},{9,21},{13,25},... | collective-permute-start | bytes 393224 | tf_op jit(solution)/shard_map/ppermute | solution.py:19
  63.3 1.3 collective-permute-start.11
  64.6 1.6 constant_dynamic-update-slice_fusion.6
  66.2 2.5 collective-permute-start.12
  68.7 1.6 constant_dynamic-update-slice_fusion.5
  71.6 1.6 constant_dynamic-update-slice_fusion.4
  73.1 6.0 %collective-permute-start.14 = (bf16[512,128]{1,0:T(8,128)(2,1)S(1)}, bf16[512,128]{1,0:T(8,128)(2,1)S(1)}, u32[]{:S(2)}, u32[]{:S(2)}) collective-permute-start(bf16[512,128]{1,0:T(8,128)(2,1)S(1)} %copy-done.3), channel_id=1, source_target_pairs={{0,8},{4,12},{8,16},{12,20},{16,24},{20,28},{1,9},{5,13},{9,17},{1... | collective-permute-start | bytes 393224 | tf_op jit(solution)/shard_map/ppermute | solution.py:19
  79.2 1.6 constant_dynamic-update-slice_fusion.3
  82.7 6.0 %collective-permute-start.16 = (bf16[512,128]{1,0:T(8,128)(2,1)S(1)}, bf16[512,128]{1,0:T(8,128)(2,1)S(1)}, u32[]{:S(2)}, u32[]{:S(2)}) collective-permute-start(bf16[512,128]{1,0:T(8,128)(2,1)S(1)} %copy-done.3), channel_id=1, source_target_pairs={{0,12},{4,16},{8,20},{12,24},{16,28},{1,13},{5,17},{9,21},{13,25},... | collective-permute-start | bytes 393224 | tf_op jit(solution)/shard_map/ppermute | solution.py:19
  94.1 3.1 collective-permute-done.17
  97.8 71.7 %while.18 = (s32[]{:T(128)}, f32[1,4,512]{2,1,0:T(4,128)S(1)}, f32[1,4,512]{2,1,0:T(4,128)S(1)}, f32[1,4,512,128]{3,2,1,0:T(8,128)}, s32[512]{0:T(512)S(1)}, /*i...) while((s32[]{:T(128)}, f32[1,4,512]{2,1,0:T(4,128)S(1)}, ...), condition=%wide.region_5.6_spmd.clone, body=%wide.region_2.5_spmd.clone.sunk | while | flops 551563264 | bytes 33431772 | solution.py:127
  98.1 3.8 %fusion.81 = (f32[4,512]{1,0:T(4,128)S(1)}, f32[512,512,4]{1,0,2:T(8,128)}) fusion(pred[512,512]{0,1:T(8,128)(4,1)S(1)} %broadcast_compare_fusion.2, bf16[512,1,4,128]{3,0,2,1:T(8,128)(2,1)S(1)} %get-tuple-element.357, bf16[3584,128]{0,1:T(8,128)(2,1)} %get-tuple-element.356, s32[]{:T(128)S(6)} %select_n.106), kind=kOutput, calls=%fused_computation.3.clone.1 | convolution fusion | flops 271579136 | bytes 5120004 | tf_op jit(solution)/shard_map/while/body/eval_jaxpr/qhgd,khd->hgqk/dot_general | solution.py:110
  101.9 4.8 %fusion.84 = f32[1,4,512,128]{3,2,1,0:T(8,128)} fusion(f32[512,512,4]{1,0,2:T(8,128)} %get-tuple-element.322, f32[4,512]{1,0:T(4,128)S(1)} %bitcast.142, pred[512,512]{0,1:T(8,128)(4,1)S(1)} %broadcast_compare_fusion.2, f32[1,4,512,128]{3,2,1,0:T(8,128)} %get-tuple-element.340, f32[4,512]{1,0:T(4,128)S(1)} %get-tuple-element.323, pred[]{:T(512)S(6)} %compare.14, ...), kind=kOutput, calls=%fused_computation.10.clone.1 | convolution fusion | flops 274464768 | bytes 6701061 | tf_op jit(solution)/shard_map/while/body/eval_jaxpr/hgqk,khd->hgqd/dot_general | solution.py:119
  108.1 3.8 %fusion.81 = (f32[4,512]{1,0:T(4,128)S(1)}, f32[512,512,4]{1,0,2:T(8,128)}) fusion(pred[512,512]{0,1:T(8,128)(4,1)S(1)} %broadcast_compare_fusion.2, bf16[512,1,4,128]{3,0,2,1:T(8,128)(2,1)S(1)} %get-tuple-element.357, bf16[3584,128]{0,1:T(8,128)(2,1)} %get-tuple-element.356, s32[]{:T(128)S(6)} %select_n.106), kind=kOutput, calls=%fused_computation.3.clone.1 | convolution fusion | flops 271579136 | bytes 5120004 | tf_op jit(solution)/shard_map/while/body/eval_jaxpr/qhgd,khd->hgqk/dot_general | solution.py:110
  111.8 5.1 %fusion.84 = f32[1,4,512,128]{3,2,1,0:T(8,128)} fusion(f32[512,512,4]{1,0,2:T(8,128)} %get-tuple-element.322, f32[4,512]{1,0:T(4,128)S(1)} %bitcast.142, pred[512,512]{0,1:T(8,128)(4,1)S(1)} %broadcast_compare_fusion.2, f32[1,4,512,128]{3,2,1,0:T(8,128)} %get-tuple-element.340, f32[4,512]{1,0:T(4,128)S(1)} %get-tuple-element.323, pred[]{:T(512)S(6)} %compare.14, ...), kind=kOutput, calls=%fused_computation.10.clone.1 | convolution fusion | flops 274464768 | bytes 6701061 | tf_op jit(solution)/shard_map/while/body/eval_jaxpr/hgqk,khd->hgqd/dot_general | solution.py:119
  118.4 3.8 %fusion.81 = (f32[4,512]{1,0:T(4,128)S(1)}, f32[512,512,4]{1,0,2:T(8,128)}) fusion(pred[512,512]{0,1:T(8,128)(4,1)S(1)} %broadcast_compare_fusion.2, bf16[512,1,4,128]{3,0,2,1:T(8,128)(2,1)S(1)} %get-tuple-element.357, bf16[3584,128]{0,1:T(8,128)(2,1)} %get-tuple-element.356, s32[]{:T(128)S(6)} %select_n.106), kind=kOutput, calls=%fused_computation.3.clone.1 | convolution fusion | flops 271579136 | bytes 5120004 | tf_op jit(solution)/shard_map/while/body/eval_jaxpr/qhgd,khd->hgqk/dot_general | solution.py:110
  122.1 5.1 %fusion.84 = f32[1,4,512,128]{3,2,1,0:T(8,128)} fusion(f32[512,512,4]{1,0,2:T(8,128)} %get-tuple-element.322, f32[4,512]{1,0:T(4,128)S(1)} %bitcast.142, pred[512,512]{0,1:T(8,128)(4,1)S(1)} %broadcast_compare_fusion.2, f32[1,4,512,128]{3,2,1,0:T(8,128)} %get-tuple-element.340, f32[4,512]{1,0:T(4,128)S(1)} %get-tuple-element.323, pred[]{:T(512)S(6)} %compare.14, ...), kind=kOutput, calls=%fused_computation.10.clone.1 | convolution fusion | flops 274464768 | bytes 6701061 | tf_op jit(solution)/shard_map/while/body/eval_jaxpr/hgqk,khd->hgqd/dot_general | solution.py:119
  128.6 3.8 %fusion.81 = (f32[4,512]{1,0:T(4,128)S(1)}, f32[512,512,4]{1,0,2:T(8,128)}) fusion(pred[512,512]{0,1:T(8,128)(4,1)S(1)} %broadcast_compare_fusion.2, bf16[512,1,4,128]{3,0,2,1:T(8,128)(2,1)S(1)} %get-tuple-element.357, bf16[3584,128]{0,1:T(8,128)(2,1)} %get-tuple-element.356, s32[]{:T(128)S(6)} %select_n.106), kind=kOutput, calls=%fused_computation.3.clone.1 | convolution fusion | flops 271579136 | bytes 5120004 | tf_op jit(solution)/shard_map/while/body/eval_jaxpr/qhgd,khd->hgqk/dot_general | solution.py:110
  132.4 5.1 %fusion.84 = f32[1,4,512,128]{3,2,1,0:T(8,128)} fusion(f32[512,512,4]{1,0,2:T(8,128)} %get-tuple-element.322, f32[4,512]{1,0:T(4,128)S(1)} %bitcast.142, pred[512,512]{0,1:T(8,128)(4,1)S(1)} %broadcast_compare_fusion.2, f32[1,4,512,128]{3,2,1,0:T(8,128)} %get-tuple-element.340, f32[4,512]{1,0:T(4,128)S(1)} %get-tuple-element.323, pred[]{:T(512)S(6)} %compare.14, ...), kind=kOutput, calls=%fused_computation.10.clone.1 | convolution fusion | flops 274464768 | bytes 6701061 | tf_op jit(solution)/shard_map/while/body/eval_jaxpr/hgqk,khd->hgqd/dot_general | solution.py:119
  138.9 3.8 %fusion.81 = (f32[4,512]{1,0:T(4,128)S(1)}, f32[512,512,4]{1,0,2:T(8,128)}) fusion(pred[512,512]{0,1:T(8,128)(4,1)S(1)} %broadcast_compare_fusion.2, bf16[512,1,4,128]{3,0,2,1:T(8,128)(2,1)S(1)} %get-tuple-element.357, bf16[3584,128]{0,1:T(8,128)(2,1)} %get-tuple-element.356, s32[]{:T(128)S(6)} %select_n.106), kind=kOutput, calls=%fused_computation.3.clone.1 | convolution fusion | flops 271579136 | bytes 5120004 | tf_op jit(solution)/shard_map/while/body/eval_jaxpr/qhgd,khd->hgqk/dot_general | solution.py:110
  142.7 5.1 %fusion.84 = f32[1,4,512,128]{3,2,1,0:T(8,128)} fusion(f32[512,512,4]{1,0,2:T(8,128)} %get-tuple-element.322, f32[4,512]{1,0:T(4,128)S(1)} %bitcast.142, pred[512,512]{0,1:T(8,128)(4,1)S(1)} %broadcast_compare_fusion.2, f32[1,4,512,128]{3,2,1,0:T(8,128)} %get-tuple-element.340, f32[4,512]{1,0:T(4,128)S(1)} %get-tuple-element.323, pred[]{:T(512)S(6)} %compare.14, ...), kind=kOutput, calls=%fused_computation.10.clone.1 | convolution fusion | flops 274464768 | bytes 6701061 | tf_op jit(solution)/shard_map/while/body/eval_jaxpr/hgqk,khd->hgqd/dot_general | solution.py:119
  149.2 3.8 %fusion.81 = (f32[4,512]{1,0:T(4,128)S(1)}, f32[512,512,4]{1,0,2:T(8,128)}) fusion(pred[512,512]{0,1:T(8,128)(4,1)S(1)} %broadcast_compare_fusion.2, bf16[512,1,4,128]{3,0,2,1:T(8,128)(2,1)S(1)} %get-tuple-element.357, bf16[3584,128]{0,1:T(8,128)(2,1)} %get-tuple-element.356, s32[]{:T(128)S(6)} %select_n.106), kind=kOutput, calls=%fused_computation.3.clone.1 | convolution fusion | flops 271579136 | bytes 5120004 | tf_op jit(solution)/shard_map/while/body/eval_jaxpr/qhgd,khd->hgqk/dot_general | solution.py:110
  153.0 5.1 %fusion.84 = f32[1,4,512,128]{3,2,1,0:T(8,128)} fusion(f32[512,512,4]{1,0,2:T(8,128)} %get-tuple-element.322, f32[4,512]{1,0:T(4,128)S(1)} %bitcast.142, pred[512,512]{0,1:T(8,128)(4,1)S(1)} %broadcast_compare_fusion.2, f32[1,4,512,128]{3,2,1,0:T(8,128)} %get-tuple-element.340, f32[4,512]{1,0:T(4,128)S(1)} %get-tuple-element.323, pred[]{:T(512)S(6)} %compare.14, ...), kind=kOutput, calls=%fused_computation.10.clone.1 | convolution fusion | flops 274464768 | bytes 6701061 | tf_op jit(solution)/shard_map/while/body/eval_jaxpr/hgqk,khd->hgqd/dot_general | solution.py:119
  159.5 3.8 %fusion.81 = (f32[4,512]{1,0:T(4,128)S(1)}, f32[512,512,4]{1,0,2:T(8,128)}) fusion(pred[512,512]{0,1:T(8,128)(4,1)S(1)} %broadcast_compare_fusion.2, bf16[512,1,4,128]{3,0,2,1:T(8,128)(2,1)S(1)} %get-tuple-element.357, bf16[3584,128]{0,1:T(8,128)(2,1)} %get-tuple-element.356, s32[]{:T(128)S(6)} %select_n.106), kind=kOutput, calls=%fused_computation.3.clone.1 | convolution fusion | flops 271579136 | bytes 5120004 | tf_op jit(solution)/shard_map/while/body/eval_jaxpr/qhgd,khd->hgqk/dot_general | solution.py:110
  163.3 5.1 %fusion.84 = f32[1,4,512,128]{3,2,1,0:T(8,128)} fusion(f32[512,512,4]{1,0,2:T(8,128)} %get-tuple-element.322, f32[4,512]{1,0:T(4,128)S(1)} %bitcast.142, pred[512,512]{0,1:T(8,128)(4,1)S(1)} %broadcast_compare_fusion.2, f32[1,4,512,128]{3,2,1,0:T(8,128)} %get-tuple-element.340, f32[4,512]{1,0:T(4,128)S(1)} %get-tuple-element.323, pred[]{:T(512)S(6)} %compare.14, ...), kind=kOutput, calls=%fused_computation.10.clone.1 | convolution fusion | flops 274464768 | bytes 6701061 | tf_op jit(solution)/shard_map/while/body/eval_jaxpr/hgqk,khd->hgqd/dot_general | solution.py:119
  169.5 1.6 fusion.45
  172.5 3.5 %all-to-all-start = ((bf16[4,128,512]{2,1,0:T(8,128)(2,1)}), bf16[4,128,512]{2,1,0:T(8,128)(2,1)S(1)}, u32[]{:S(2)}, u32[]{:S(2)}) async-start(bf16[4,128,512]{2,1,0:T(8,128)(2,1)} %convert_element_type.95), calls=%async_computation | async-start | bytes 1048576 | tf_op jit(solution)/shard_map/all_to_all | solution.py:131
  176.3 8.5 %all-to-all-done = bf16[4,128,512]{2,1,0:T(8,128)(2,1)S(1)} async-done(((bf16[4,128,512]{2,1,0:T(8,128)(2,1)}), bf16[4,128,512]{2,1,0:T(8,128)(2,1)S(1)}, u32[]{:S(2)}, u32[]{:S(2)}) %all-to-all-start) | async-done | bytes 524320 | tf_op jit(solution)/shard_map/all_to_all | solution.py:131
  185.7 4.9 %multiply_reduce_fusion.1 = (f32[128]{0:T(128)S(1)}, f32[128,2048]{1,0:T(8,128)S(1)}) fusion(bf16[128,2048]{0,1:T(8,128)(2,1)} %bitcast.141, bf16[2048,2048]{1,0:T(8,128)(2,1)} %param.23, bf16[128,2048]{1,0:T(8,128)(2,1)} %param.16), kind=kOutput, calls=%fused_computation.48 | convolution fusion | flops 1075314560 | bytes 10486272 | tf_op jit(solution)/shard_map/dot_general | solution.py:132
  191.5 53.0 %all_to_all.26 = bf16[32,16,2048]{2,1,0:T(8,128)(2,1)S(1)} all-to-all(bf16[32,16,2048]{2,1,0:T(8,128)(2,1)S(1)} %bitcast.140), channel_id=1, replica_groups=mesh['sp'=8,'tp'=4] {'sp','tp'}, dimensions={0} | all-to-all | bytes 4194304 | tf_op jit(solution)/shard_map/all_to_all | solution.py:158
  244.5 1.3 copy-done.2
  245.8 2.2 fusion.30
  248.1 6.3 %convolution_convert_fusion.1 = bf16[512,2048]{1,0:T(8,128)(2,1)} fusion(bf16[1,512,2048]{2,1,0:T(8,128)(2,1)S(1)} %copy-done, bf16[512,2048]{1,0:T(8,128)(2,1)} %bitcast.146, bf16[1,2048,512]{2,1,0:T(8,128)(2,1)} %param.28, f32[512,512]{1,0:T(8,128)} %fusion.30), kind=kOutput, calls=%fused_computation.30 | convolution fusion | flops 2150105088 | bytes 9437184 | tf_op jit(solution)/shard_map/dot_general | solution.py:164
  254.3 3.8 %all-to-all-start.2 = ((bf16[32,16,2048]{2,1,0:T(8,128)(2,1)}), bf16[32,16,2048]{2,1,0:T(8,128)(2,1)}, u32[]{:S(2)}, u32[]{:S(2)}) async-start(bf16[32,16,2048]{2,1,0:T(8,128)(2,1)} %bitcast.144), calls=%async_computation.2 | async-start | bytes 4194304 | tf_op jit(solution)/shard_map/all_to_all | solution.py:167
  258.4 48.4 %all-to-all-done.2 = bf16[32,16,2048]{2,1,0:T(8,128)(2,1)} async-done(((bf16[32,16,2048]{2,1,0:T(8,128)(2,1)}), bf16[32,16,2048]{2,1,0:T(8,128)(2,1)}, u32[]{:S(2)}, u32[]{:S(2)}) %all-to-all-start.2) | async-done | bytes 2097184 | tf_op jit(solution)/shard_map/all_to_all | solution.py:167
  306.8 5.2 %gather_fusion = bf16[256,2048]{1,0:T(8,128)(2,1)} fusion(bf16[512,2048]{1,0:T(8,128)(2,1)} %bitcast.19, s32[1024]{0:T(1024)S(1)} %pad_clamp_fusion), kind=kCustom, calls=%fused_computation | custom fusion | bytes 2098176 | tf_op jit(solution)/shard_map/gather | solution.py:174
  312.0 3.4 %reshape.419 = f32[128,2,2048]{2,1,0:T(2,128)} reshape(bf16[256,2048]{1,0:T(8,128)(2,1)} %gather_fusion) | data formatting | bytes 3145728 | tf_op jit(solution)/shard_map/convert_element_type | solution.py:175
  315.4 4.8 %multiply_reduce_fusion = f32[128,2048]{1,0:T(8,128)S(1)} fusion(f32[128,2,2048]{2,1,0:T(2,128)} %reshape.419, f32[128,2]{1,0:T(8,128)S(1)} %copy.55), kind=kLoop, calls=%fused_computation.39 | loop fusion | flops 786432 | bytes 3146752 | tf_op jit(solution)/shard_map/reduce_sum | solution.py:176
  (151 shorter events, 39.7 us)
Async XLA Ops:
  0.0 248.1 %copy-start = (bf16[1,512,2048]{2,1,0:T(8,128)(2,1)S(1)}, bf16[1,512,2048]{2,1,0:T(8,128)(2,1)}, u32[]{:S(2)}) copy-start(bf16[1,512,2048]{2,1,0:T(8,128)(2,1)} %param.29) | copy-start | bytes 6291460
  0.0 25.5 %copy-start.6 = (f32[128]{0:T(128)S(1)}, f32[128]{0:T(128)}, u32[]{:S(2)}) copy-start(f32[128]{0:T(128)} %param.20) | copy-start | bytes 1540
  2.6 60.6 %collective-permute-start.6 = (bf16[512,128]{0,1:T(8,128)(2,1)S(1)}, bf16[512,128]{0,1:T(8,128)(2,1)}, u32[]{:S(2)}, u32[]{:S(2)}) collective-permute-start(bf16[512,128]{0,1:T(8,128)(2,1)S(1)} %maximum_bitcast_fusion), channel_id=1, source_target_pairs={{0,4},{4,8},{8,12},{12,16},{16,20},{20,24},{24,28},{1,5},{5,9},{9,... | collective-permute-start | bytes 393224 | tf_op jit(solution)/shard_map/ppermute | solution.py:19
  8.2 58.0 %collective-permute-start.7 = (bf16[512,128]{0,1:T(8,128)(2,1)S(1)}, bf16[512,128]{0,1:T(8,128)(2,1)}, u32[]{:S(2)}, u32[]{:S(2)}) collective-permute-start(bf16[512,128]{0,1:T(8,128)(2,1)S(1)} %maximum_bitcast_fusion), channel_id=1, source_target_pairs={{4,0},{8,4},{12,8},{16,12},{20,16},{24,20},{28,24},{5,1},{9,5},{13... | collective-permute-start | bytes 393224 | tf_op jit(solution)/shard_map/ppermute | solution.py:19
  9.5 60.8 %collective-permute-start.8 = (bf16[512,128]{0,1:T(8,128)(2,1)S(1)}, bf16[512,128]{0,1:T(8,128)(2,1)}, u32[]{:S(2)}, u32[]{:S(2)}) collective-permute-start(bf16[512,128]{0,1:T(8,128)(2,1)S(1)} %maximum_bitcast_fusion), channel_id=1, source_target_pairs={{0,8},{4,12},{8,16},{12,20},{16,24},{20,28},{1,9},{5,13},{9,17},{1... | collective-permute-start | bytes 393224 | tf_op jit(solution)/shard_map/ppermute | solution.py:19
  15.0 58.2 %collective-permute-start.9 = (bf16[512,128]{0,1:T(8,128)(2,1)S(1)}, bf16[512,128]{0,1:T(8,128)(2,1)}, u32[]{:S(2)}, u32[]{:S(2)}) collective-permute-start(bf16[512,128]{0,1:T(8,128)(2,1)S(1)} %maximum_bitcast_fusion), channel_id=1, source_target_pairs={{8,0},{12,4},{16,8},{20,12},{24,16},{28,20},{9,1},{13,5},{17,9},{2... | collective-permute-start | bytes 393224 | tf_op jit(solution)/shard_map/ppermute | solution.py:19
  17.0 9.3 %collective-permute-start = (s32[512]{0:T(512)S(1)}, s32[512]{0:T(512)S(1)}, u32[]{:S(2)}, u32[]{:S(2)}) collective-permute-start(s32[512]{0:T(512)S(1)} %get-tuple-element.328), channel_id=1, source_target_pairs={{0,4},{4,8},{8,12},{12,16},{16,20},{20,24},{24,28},{1,5},{5,9},{9,... | collective-permute-start | bytes 6152 | tf_op jit(solution)/shard_map/ppermute | solution.py:19
  21.0 45.2 %copy-start.3 = (bf16[512,128]{1,0:T(8,128)(2,1)S(1)}, bf16[512,128]{1,0:T(8,128)(2,1)}, u32[]{:S(2)}) copy-start(bf16[512,128]{1,0:T(8,128)(2,1)} %param.19) | copy-start | bytes 393220
  26.3 7.0 %collective-permute-start.1 = (s32[512]{0:T(512)S(1)}, s32[512]{0:T(512)S(1)}, u32[]{:S(2)}, u32[]{:S(2)}) collective-permute-start(s32[512]{0:T(512)S(1)} %get-tuple-element.328), channel_id=1, source_target_pairs={{4,0},{8,4},{12,8},{16,12},{20,16},{24,20},{28,24},{5,1},{9,5},{13... | collective-permute-start | bytes 6152 | tf_op jit(solution)/shard_map/ppermute | solution.py:19
  33.3 4.4 %collective-permute-start.2 = (s32[512]{0:T(512)S(1)}, s32[512]{0:T(512)S(1)}, u32[]{:S(2)}, u32[]{:S(2)}) collective-permute-start(s32[512]{0:T(512)S(1)} %get-tuple-element.328), channel_id=1, source_target_pairs={{0,8},{4,12},{8,16},{12,20},{16,24},{20,28},{1,9},{5,13},{9,17},{1... | collective-permute-start | bytes 6152 | tf_op jit(solution)/shard_map/ppermute | solution.py:19
  37.7 5.7 %collective-permute-start.3 = (s32[512]{0:T(512)S(1)}, s32[512]{0:T(512)S(1)}, u32[]{:S(2)}, u32[]{:S(2)}) collective-permute-start(s32[512]{0:T(512)S(1)} %get-tuple-element.328), channel_id=1, source_target_pairs={{8,0},{12,4},{16,8},{20,12},{24,16},{28,20},{9,1},{13,5},{17,9},{2... | collective-permute-start | bytes 6152 | tf_op jit(solution)/shard_map/ppermute | solution.py:19
  43.4 7.5 %collective-permute-start.4 = (s32[512]{0:T(512)S(1)}, s32[512]{0:T(512)S(1)}, u32[]{:S(2)}, u32[]{:S(2)}) collective-permute-start(s32[512]{0:T(512)S(1)} %get-tuple-element.328), channel_id=1, source_target_pairs={{0,12},{4,16},{8,20},{12,24},{16,28},{1,13},{5,17},{9,21},{13,25},... | collective-permute-start | bytes 6152 | tf_op jit(solution)/shard_map/ppermute | solution.py:19
  50.9 6.6 %collective-permute-start.5 = (s32[512]{0:T(512)S(1)}, s32[512]{0:T(512)S(1)}, u32[]{:S(2)}, u32[]{:S(2)}) collective-permute-start(s32[512]{0:T(512)S(1)} %get-tuple-element.328), channel_id=1, source_target_pairs={{12,0},{16,4},{20,8},{24,12},{28,16},{13,1},{17,5},{21,9},{25,13},... | collective-permute-start | bytes 6152 | tf_op jit(solution)/shard_map/ppermute | solution.py:19
  57.5 23.2 %collective-permute-start.10 = (bf16[512,128]{0,1:T(8,128)(2,1)S(1)}, bf16[512,128]{0,1:T(8,128)(2,1)S(1)}, u32[]{:S(2)}, u32[]{:S(2)}) collective-permute-start(bf16[512,128]{0,1:T(8,128)(2,1)S(1)} %maximum_bitcast_fusion), channel_id=1, source_target_pairs={{0,12},{4,16},{8,20},{12,24},{16,28},{1,13},{5,17},{9,21},{13,25},... | collective-permute-start | bytes 393224 | tf_op jit(solution)/shard_map/ppermute | solution.py:19
  63.3 19.5 %collective-permute-start.11 = (bf16[512,128]{0,1:T(8,128)(2,1)S(1)}, bf16[512,128]{0,1:T(8,128)(2,1)S(1)}, u32[]{:S(2)}, u32[]{:S(2)}) collective-permute-start(bf16[512,128]{0,1:T(8,128)(2,1)S(1)} %maximum_bitcast_fusion), channel_id=1, source_target_pairs={{12,0},{16,4},{20,8},{24,12},{28,16},{13,1},{17,5},{21,9},{25,13},... | collective-permute-start | bytes 393224 | tf_op jit(solution)/shard_map/ppermute | solution.py:19
  66.2 23.2 %collective-permute-start.12 = (bf16[512,128]{1,0:T(8,128)(2,1)S(1)}, bf16[512,128]{1,0:T(8,128)(2,1)S(1)}, u32[]{:S(2)}, u32[]{:S(2)}) collective-permute-start(bf16[512,128]{1,0:T(8,128)(2,1)S(1)} %copy-done.3), channel_id=1, source_target_pairs={{0,4},{4,8},{8,12},{12,16},{16,20},{20,24},{24,28},{1,5},{5,9},{9,... | collective-permute-start | bytes 393224 | tf_op jit(solution)/shard_map/ppermute | solution.py:19
  70.3 21.1 %collective-permute-start.13 = (bf16[512,128]{1,0:T(8,128)(2,1)S(1)}, bf16[512,128]{1,0:T(8,128)(2,1)S(1)}, u32[]{:S(2)}, u32[]{:S(2)}) collective-permute-start(bf16[512,128]{1,0:T(8,128)(2,1)S(1)} %copy-done.3), channel_id=1, source_target_pairs={{4,0},{8,4},{12,8},{16,12},{20,16},{24,20},{28,24},{5,1},{9,5},{13... | collective-permute-start | bytes 393224 | tf_op jit(solution)/shard_map/ppermute | solution.py:19
  73.1 18.9 %collective-permute-start.14 = (bf16[512,128]{1,0:T(8,128)(2,1)S(1)}, bf16[512,128]{1,0:T(8,128)(2,1)S(1)}, u32[]{:S(2)}, u32[]{:S(2)}) collective-permute-start(bf16[512,128]{1,0:T(8,128)(2,1)S(1)} %copy-done.3), channel_id=1, source_target_pairs={{0,8},{4,12},{8,16},{12,20},{16,24},{20,28},{1,9},{5,13},{9,17},{1... | collective-permute-start | bytes 393224 | tf_op jit(solution)/shard_map/ppermute | solution.py:19
  80.7 12.0 %collective-permute-start.15 = (bf16[512,128]{1,0:T(8,128)(2,1)S(1)}, bf16[512,128]{1,0:T(8,128)(2,1)S(1)}, u32[]{:S(2)}, u32[]{:S(2)}) collective-permute-start(bf16[512,128]{1,0:T(8,128)(2,1)S(1)} %copy-done.3), channel_id=1, source_target_pairs={{8,0},{12,4},{16,8},{20,12},{24,16},{28,20},{9,1},{13,5},{17,9},{2... | collective-permute-start | bytes 393224 | tf_op jit(solution)/shard_map/ppermute | solution.py:19
  82.7 10.7 %collective-permute-start.16 = (bf16[512,128]{1,0:T(8,128)(2,1)S(1)}, bf16[512,128]{1,0:T(8,128)(2,1)S(1)}, u32[]{:S(2)}, u32[]{:S(2)}) collective-permute-start(bf16[512,128]{1,0:T(8,128)(2,1)S(1)} %copy-done.3), channel_id=1, source_target_pairs={{0,12},{4,16},{8,20},{12,24},{16,28},{1,13},{5,17},{9,21},{13,25},... | collective-permute-start | bytes 393224 | tf_op jit(solution)/shard_map/ppermute | solution.py:19
  89.4 7.7 %collective-permute-start.17 = (bf16[512,128]{1,0:T(8,128)(2,1)S(1)}, bf16[512,128]{1,0:T(8,128)(2,1)S(1)}, u32[]{:S(2)}, u32[]{:S(2)}) collective-permute-start(bf16[512,128]{1,0:T(8,128)(2,1)S(1)} %copy-done.3), channel_id=1, source_target_pairs={{12,0},{16,4},{20,8},{24,12},{28,16},{13,1},{17,5},{21,9},{25,13},... | collective-permute-start | bytes 393224 | tf_op jit(solution)/shard_map/ppermute | solution.py:19
  101.9 4.8 %copy-start.1 = (f32[512,512,4]{1,0,2:T(8,128)S(1)}, f32[512,512,4]{1,0,2:T(8,128)}, u32[]{:S(2)}) copy-start(f32[512,512,4]{1,0,2:T(8,128)} %get-tuple-element.322) | copy-start | bytes 12582916 | tf_op jit(solution)/shard_map/while
  111.8 5.1 %copy-start.1 = (f32[512,512,4]{1,0,2:T(8,128)S(1)}, f32[512,512,4]{1,0,2:T(8,128)}, u32[]{:S(2)}) copy-start(f32[512,512,4]{1,0,2:T(8,128)} %get-tuple-element.322) | copy-start | bytes 12582916 | tf_op jit(solution)/shard_map/while
  122.1 5.1 %copy-start.1 = (f32[512,512,4]{1,0,2:T(8,128)S(1)}, f32[512,512,4]{1,0,2:T(8,128)}, u32[]{:S(2)}) copy-start(f32[512,512,4]{1,0,2:T(8,128)} %get-tuple-element.322) | copy-start | bytes 12582916 | tf_op jit(solution)/shard_map/while
  132.4 5.1 %copy-start.1 = (f32[512,512,4]{1,0,2:T(8,128)S(1)}, f32[512,512,4]{1,0,2:T(8,128)}, u32[]{:S(2)}) copy-start(f32[512,512,4]{1,0,2:T(8,128)} %get-tuple-element.322) | copy-start | bytes 12582916 | tf_op jit(solution)/shard_map/while
  142.7 5.1 %copy-start.1 = (f32[512,512,4]{1,0,2:T(8,128)S(1)}, f32[512,512,4]{1,0,2:T(8,128)}, u32[]{:S(2)}) copy-start(f32[512,512,4]{1,0,2:T(8,128)} %get-tuple-element.322) | copy-start | bytes 12582916 | tf_op jit(solution)/shard_map/while
  153.0 5.1 %copy-start.1 = (f32[512,512,4]{1,0,2:T(8,128)S(1)}, f32[512,512,4]{1,0,2:T(8,128)}, u32[]{:S(2)}) copy-start(f32[512,512,4]{1,0,2:T(8,128)} %get-tuple-element.322) | copy-start | bytes 12582916 | tf_op jit(solution)/shard_map/while
  163.3 5.1 %copy-start.1 = (f32[512,512,4]{1,0,2:T(8,128)S(1)}, f32[512,512,4]{1,0,2:T(8,128)}, u32[]{:S(2)}) copy-start(f32[512,512,4]{1,0,2:T(8,128)} %get-tuple-element.322) | copy-start | bytes 12582916 | tf_op jit(solution)/shard_map/while
  172.5 12.3 %all-to-all-start = ((bf16[4,128,512]{2,1,0:T(8,128)(2,1)}), bf16[4,128,512]{2,1,0:T(8,128)(2,1)S(1)}, u32[]{:S(2)}, u32[]{:S(2)}) async-start(bf16[4,128,512]{2,1,0:T(8,128)(2,1)} %convert_element_type.95), calls=%async_computation | async-start | bytes 1048576 | tf_op jit(solution)/shard_map/all_to_all | solution.py:131
  185.7 5.0 %copy-start.4 = (f32[2048]{0:T(1024)S(1)}, f32[2048]{0:T(1024)}, u32[]{:S(2)}) copy-start(f32[2048]{0:T(1024)} %param.24) | copy-start | bytes 24580
  190.7 55.1 %copy-start.7 = (bf16[1,2048,512]{2,1,0:T(8,128)(2,1)S(1)}, bf16[1,2048,512]{2,1,0:T(8,128)(2,1)}, u32[]{:S(2)}) copy-start(bf16[1,2048,512]{2,1,0:T(8,128)(2,1)} %param.27) | copy-start | bytes 6291460
  244.5 1.3 copy-start.2
  254.3 3.9 %copy-start.5 = (f32[128,2]{0,1:T(2,128)S(1)}, f32[128,2]{0,1:T(2,128)}, u32[]{:S(2)}) copy-start(f32[128,2]{0,1:T(2,128)} %param.26) | copy-start | bytes 3076
  254.3 52.5 %all-to-all-start.2 = ((bf16[32,16,2048]{2,1,0:T(8,128)(2,1)}), bf16[32,16,2048]{2,1,0:T(8,128)(2,1)}, u32[]{:S(2)}, u32[]{:S(2)}) async-start(bf16[32,16,2048]{2,1,0:T(8,128)(2,1)} %bitcast.144), calls=%async_computation.2 | async-start | bytes 4194304 | tf_op jit(solution)/shard_map/all_to_all | solution.py:167
where the time goes:
time: 322 us; the launch traced here: 321 us
  waiting for transfers between devices  78 us (24%)
  matrix products  75.9 us (24%)
  starting transfers between devices  61.9 us (19%)
  blocking collectives  53 us (16%)
  local copies, waits for them, and re-layouts  30.6 us (10%)
  other arithmetic  21 us (7%)
    ppermute x18, starting transfers between devices, from_behind(): return lax.ppermute(block, axis, route)  54.7 us
    all_to_all x1, blocking collectives, on_device(): lax.all_to_all(outgoing, ('sp', 'tp'), split_axis=0, concat_axis=0, tiled...  53 us
    all_to_all x1, waiting for transfers between devices, on_device(): lax.all_to_all(expert_out.reshape(sources, slots, width), ('sp', 'tp'), s...  48.4 us
    dot_general x7, matrix products, one_block(): jnp.einsum('hgqk,khd->hgqd', weights.astype(jnp.bfloat16), value_block, p...  35.4 us
    dot_general x7, matrix products, one_block(): jnp.einsum('qhgd,khd->hgqk', query_grid, key_block, preferred_element_typ...  26.3 us
    ppermute x18, waiting for transfers between devices, from_behind(): return lax.ppermute(block, axis, route)  21.1 us
    unnamed x35, local copies, waits for them, and re-layouts  16.9 us
    all_to_all x1, waiting for transfers between devices, on_device(): lax.all_to_all(attn, 'tp', split_axis=0, concat_axis=1, tiled=True)  8.46 us
  transfers between devices with their start and end apart: 20, of which 8 were waited for; matrix products, arithmetic and copies ran while one was open for 6% of the time, Pallas kernels for 0%

commit v1 on v0

v1 whole, which is shorter than its diff:
```python
import functools
import math

import jax
import jax.numpy as jnp
from jax import lax
from jax.experimental import pallas as pl
from jax.experimental.pallas import tpu as pltpu
from jax.sharding import PartitionSpec as P

HEAD = 128
GRID_W = 64
REACH = 3


norm_eps = 1e-06
rope_base = 10000.0
masked_low = -1e30
MESH = pl.DeviceIdType.MESH
DOC_KEY = 128.0
DOC_QUERY = 64.0
EXP2_SCALE = math.log2(math.e) / math.sqrt(HEAD)


def rotary_tables(first_row, length):
    freq_count = HEAD // 4
    inverse = 1.0 / rope_base ** (jnp.arange(freq_count, dtype=jnp.float32) / freq_count)
    position = first_row + jnp.arange(length, dtype=jnp.int32)
    grid_row = (position // GRID_W).astype(jnp.float32)
    grid_col = (position % GRID_W).astype(jnp.float32)
    angles = jnp.concatenate(
        [grid_row[:, None] * inverse[None, :], grid_col[:, None] * inverse[None, :]], axis=1
    )
    return (jnp.cos(angles), jnp.sin(angles))


def norm_rotate(projected, gains, cosine, sine_table):
    length = projected.shape[0]
    values_wide = projected.astype(jnp.float32).reshape(length, -1, HEAD)
    scaled = (
        values_wide
        * lax.rsqrt(jnp.mean(values_wide * values_wide, axis=-1, keepdims=True) + norm_eps)
        * gains
    )
    half_size = HEAD // 2
    first_half = scaled[..., :half_size]
    second_half = scaled[..., half_size:]
    cosine_rows = cosine[:, None, :]
    sine_rows = sine_table[:, None, :]
    turned = jnp.concatenate(
        [
            first_half * cosine_rows - second_half * sine_rows,
            first_half * sine_rows + second_half * cosine_rows,
        ],
        axis=-1,
    )
    return turned.reshape(length, -1).astype(jnp.bfloat16)


def attention_kernel(
    n_sp, n_tp, q_ref, k_ref, vt_ref, doc_ref, res_ref, gain_ref, wo_hbm,
    hid_ref, nrm_ref,
    wo_v, k_in, vt_in, doc_in, k_aug, m_s, l_s, acc_s, att_s, all_s,
    send, recv, t_send, t_recv, w_sem,
):
    sp = lax.axis_index("sp")
    tp = lax.axis_index("tp")
    heads = q_ref.shape[0]
    rows = res_ref.shape[0]
    width = att_s.shape[1]
    slots = 2 * REACH

    def distance(j):
        return (j // 2 + 1) * (1 - 2 * (j % 2))

    def inside(index):
        return jnp.logical_and(index >= 0, index < n_sp)

    wo_copy = pltpu.make_async_copy(wo_hbm, wo_v, w_sem)
    wo_copy.start()

    barrier = pltpu.get_barrier_semaphore()
    for j in range(slots):
        there = sp + distance(j)

        @pl.when(inside(there))
        def _():
            pl.semaphore_signal(barrier, inc=1, device_id=(there, tp), device_id_type=MESH)

    for k in range(1, n_tp):
        pl.semaphore_signal(
            barrier, inc=1, device_id=(sp, lax.rem(tp + k, n_tp)), device_id_type=MESH
        )
    beside = jnp.minimum(sp, REACH) + jnp.minimum(n_sp - 1 - sp, REACH)
    pl.semaphore_wait(barrier, n_tp - 1 + beside)

    def copies(j):
        there = (sp + distance(j), tp)
        return [
            pltpu.make_async_remote_copy(
                src_ref=one,
                dst_ref=into.at[j],
                send_sem=send.at[j, i],
                recv_sem=recv.at[j, i],
                device_id=there,
                device_id_type=MESH,
            )
            for i, (one, into) in enumerate(((k_ref, k_in), (vt_ref, vt_in), (doc_ref, doc_in)))
        ]

    for j in range(slots):

        @pl.when(inside(sp + distance(j)))
        def _():
            for copy in copies(j):
                copy.start()

    def take(keys, values_t, docs, first):
        length = keys.shape[0]
        doc_col = jnp.broadcast_to(docs[0:1, :], (HEAD, length)).T
        lanes = lax.broadcasted_iota(jnp.int32, (length, HEAD), 1).astype(jnp.float32)
        k_aug[:, :HEAD] = keys[...]
        k_aug[:, HEAD:] = jnp.where(doc_col == lanes, DOC_KEY, 0.0).astype(jnp.bfloat16)
        for h in range(heads):
            s = jnp.dot(k_aug[...], q_ref[h], preferred_element_type=jnp.float32)
            top = jnp.max(s, axis=0, keepdims=True)
            if not first:
                top = jnp.maximum(m_s[h], top)
            e = jnp.exp2((s - top) * EXP2_SCALE)
            den = jnp.sum(e, axis=0, keepdims=True)
            part = jnp.dot(
                values_t[...], e.astype(jnp.bfloat16), preferred_element_type=jnp.float32
            )
            if first:
                l_s[h] = den
                acc_s[h] = part
            else:
                old = jnp.exp2((m_s[h] - top) * EXP2_SCALE)
                l_s[h] = l_s[h] * old + den
                acc_s[h] = acc_s[h] * old + part
            m_s[h] = top

    take(k_ref, vt_ref, doc_ref, True)

    def step(j, carry):
        @pl.when(inside(sp - distance(j)))
        def _():
            for copy in copies(j):
                copy.wait_recv()
            take(k_in.at[j], vt_in.at[j], doc_in.at[j], False)

        return carry

    lax.fori_loop(0, slots, step, 0)

    for h in range(heads):
        out = acc_s[h] / l_s[h]
        att_s[:, h * HEAD : (h + 1) * HEAD] = out.T.astype(jnp.bfloat16)

    def exchange(k):
        there = lax.rem(tp + k, n_tp)
        return pltpu.make_async_remote_copy(
            src_ref=att_s.at[pl.ds(pl.multiple_of(there * rows, rows), rows), :],
            dst_ref=all_s.at[tp],
            send_sem=t_send.at[k],
            recv_sem=t_recv.at[k],
            device_id=(sp, there),
            device_id_type=MESH,
        )

    for k in range(n_tp - 1, 0, -1):
        exchange(k).start()
    wo_copy.wait()

    def weight_rows(i):
        return wo_v[pl.ds(pl.multiple_of(i * width, width), width), :]

    projected = jnp.dot(
        att_s[pl.ds(pl.multiple_of(tp * rows, rows), rows), :],
        weight_rows(tp),
        preferred_element_type=jnp.float32,
    )
    for k in range(1, n_tp):
        exchange(k).wait_recv()
        source = lax.rem(tp - k + n_tp, n_tp)
        projected += jnp.dot(
            all_s[source], weight_rows(source), preferred_element_type=jnp.float32
        )
    hidden = (res_ref[...].astype(jnp.float32) + projected).astype(jnp.bfloat16)
    hid_ref[...] = hidden
    wide = hidden.astype(jnp.float32)
    mean = jnp.mean(wide * wide, axis=-1, keepdims=True)
    nrm_ref[...] = (wide * lax.rsqrt(mean + norm_eps) * gain_ref[...]).astype(jnp.bfloat16)

    for j in range(slots):

        @pl.when(inside(sp + distance(j)))
        def _():
            for copy in copies(j):
                copy.wait_send()

    for k in range(1, n_tp):
        exchange(k).wait_send()


def attend(q_aug, key_norm, value_t, doc_rows, residual, norm_gain, output_weight):
    n_sp, n_tp = lax.axis_size("sp"), lax.axis_size("tp")
    heads, deep, length = q_aug.shape
    rows, model = residual.shape
    vmem = pl.BlockSpec(memory_space=pltpu.VMEM)
    slots = 2 * REACH
    return pl.pallas_call(
        functools.partial(attention_kernel, n_sp, n_tp),
        out_shape=[jax.ShapeDtypeStruct((rows, model), jnp.bfloat16)] * 2,
        in_specs=[vmem] * 6 + [pl.BlockSpec(memory_space=pl.ANY)],
        out_specs=[vmem] * 2,
        scratch_shapes=[
            pltpu.VMEM(output_weight.shape, jnp.bfloat16),
            pltpu.VMEM((slots,) + key_norm.shape, jnp.bfloat16),
            pltpu.VMEM((slots,) + value_t.shape, jnp.bfloat16),
            pltpu.VMEM((slots,) + doc_rows.shape, jnp.float32),
            pltpu.VMEM((length, deep), jnp.bfloat16),
            pltpu.VMEM((heads, 1, length), jnp.float32),
            pltpu.VMEM((heads, 1, length), jnp.float32),
            pltpu.VMEM((heads, HEAD, length), jnp.float32),
            pltpu.VMEM((length, heads * HEAD), jnp.bfloat16),
            pltpu.VMEM((n_tp, rows, heads * HEAD), jnp.bfloat16),
            pltpu.SemaphoreType.DMA((slots, 3)),
            pltpu.SemaphoreType.DMA((slots, 3)),
            pltpu.SemaphoreType.DMA((n_tp,)),
            pltpu.SemaphoreType.DMA((n_tp,)),
            pltpu.SemaphoreType.DMA(()),
        ],
        compiler_params=pltpu.CompilerParams(
            collective_id=1, has_side_effects=True, vmem_limit_bytes=48 * 1024 * 1024
        ),
    )(q_aug, key_norm, value_t, doc_rows, residual, norm_gain.reshape(1, -1), output_weight)


def on_device(
    residual,
    query_proj,
    key_proj,
    value_proj,
    query_gain,
    key_gain,
    document_ids,
    output_weight,
    norm_gain,
    expert_ids,
    route_weights,
    gate_weight,
    up_weight,
    down_weight,
):
    rows_here = query_proj.shape[0]
    cosine, sine_table = rotary_tables(lax.axis_index("sp") * rows_here, rows_here)
    query_norm = norm_rotate(query_proj, query_gain, cosine, sine_table)
    key_norm = norm_rotate(key_proj, key_gain, cosine, sine_table)
    heads = query_proj.shape[1] // HEAD
    docs = document_ids.astype(jnp.float32)
    query_t = jnp.transpose(query_norm.reshape(rows_here, heads, HEAD), (1, 2, 0))
    query_doc = jnp.where(
        docs[None, :] == jnp.arange(HEAD, dtype=jnp.float32)[:, None], DOC_QUERY, 0.0
    ).astype(jnp.bfloat16)
    q_aug = jnp.concatenate(
        [query_t, jnp.broadcast_to(query_doc[None], (heads, HEAD, rows_here))], axis=1
    )
    doc_rows = jnp.broadcast_to(docs[None, :], (8, rows_here))
    hidden, normed = attend(
        q_aug, key_norm, value_proj.T, doc_rows, residual, norm_gain, output_weight
    )
    token_rows = residual.shape[0]
    top_count = expert_ids.shape[1]
    experts_all = lax.axis_size("sp") * lax.axis_size("tp")
    capacity = max(2, 2 * token_rows * top_count // experts_all)
    flat_ids = expert_ids.reshape(-1)
    onehot = (flat_ids[:, None] == jnp.arange(experts_all, dtype=jnp.int32)[None, :]).astype(
        jnp.int32
    )
    arrival = jnp.sum(jnp.cumsum(onehot, axis=0) * onehot, axis=1) - 1
    slot_index = flat_ids * capacity + arrival
    slot_grid = slot_index.reshape(token_rows, top_count)
    placing = jnp.sum(
        (
            jnp.arange(experts_all * capacity, dtype=jnp.int32)[:, None, None] == slot_grid[None]
        ).astype(jnp.float32),
        axis=2,
    ).astype(jnp.bfloat16)
    outgoing = jnp.dot(placing, normed, preferred_element_type=jnp.float32).astype(jnp.bfloat16)
    outgoing = outgoing.reshape(experts_all, capacity, normed.shape[1])
    arrived = lax.all_to_all(outgoing, ("sp", "tp"), split_axis=0, concat_axis=0, tiled=True)
    sources, slots, width = arrived.shape
    flat_rows = arrived.reshape(sources * slots, width)
    gate_part = jnp.dot(flat_rows, gate_weight[0], preferred_element_type=jnp.float32)
    up_part = jnp.dot(flat_rows, up_weight[0], preferred_element_type=jnp.float32)
    activity = (jax.nn.silu(gate_part) * up_part).astype(jnp.bfloat16)
    expert_out = jnp.dot(activity, down_weight[0], preferred_element_type=jnp.float32).astype(
        jnp.bfloat16
    )
    returned = lax.all_to_all(
        expert_out.reshape(sources, slots, width),
        ("sp", "tp"),
        split_axis=0,
        concat_axis=0,
        tiled=True,
    )
    spread = jnp.sum(
        jnp.where(
            jnp.arange(experts_all * capacity, dtype=jnp.int32)[None, None, :]
            == slot_grid[:, :, None],
            route_weights[:, :, None],
            0.0,
        ),
        axis=1,
    )
    high = spread.astype(jnp.bfloat16)
    low = (spread - high.astype(jnp.float32)).astype(jnp.bfloat16)
    rows_back = returned.reshape(experts_all * capacity, -1)
    combined = jnp.dot(high, rows_back, preferred_element_type=jnp.float32) + jnp.dot(
        low, rows_back, preferred_element_type=jnp.float32
    )
    return (hidden.astype(jnp.float32) + combined).astype(jnp.bfloat16)


def solution(mesh):
    in_specs = (
        P(("sp", "tp"), None),
        P("sp", "tp"),
        P("sp", "tp"),
        P("sp", "tp"),
        P(),
        P(),
        P("sp"),
        P(),
        P(),
        P(("sp", "tp"), None),
        P(("sp", "tp"), None),
        P(("sp", "tp"), None, None),
        P(("sp", "tp"), None, None),
        P(("sp", "tp"), None, None),
    )
    out_specs = P(("sp", "tp"), None)
    return jax.shard_map(
        on_device, mesh=mesh, in_specs=in_specs, out_specs=out_specs, check_vma=False
    )
```

time: 322 us -> 194 us (0.60)
  matrix products: 75.9 us -> 14.1 us
  starting transfers between devices: 61.9 us -> 3.79 us
  Pallas kernels: 0 us -> 31.2 us
  waiting for transfers between devices: 78 us -> 48.6 us
  local copies, waits for them, and re-layouts: 30.6 us -> 11.5 us
  blocking collectives: 53 us -> 71.4 us
  other arithmetic: 21 us -> 12.7 us
    dot_general x15 -> x2, matrix products: 66.6 us -> 4.88 us  [the longest x1 2.85 us: on_device(): jnp.dot(low, rows_back, preferred_element_type=jnp.float32)]
    ppermute x18 -> x0, starting transfers between devices: 54.7 us -> none  [from_behind(): return lax.ppermute(block, axis, route)]
    pallas_call x0 -> x1, Pallas kernels: none -> 31.2 us  [attend(): pl.pallas_call(functools.partial(attention_kernel, n_sp, n_tp), out_shape...]
    ppermute x18 -> x0, waiting for transfers between devices: 21.1 us -> none  [from_behind(): return lax.ppermute(block, axis, route)]
    all_to_all x1, blocking collectives: 53 us -> 71.4 us  [on_device(): lax.all_to_all(outgoing, ('sp', 'tp'), split_axis=0, concat_axis=0, tiled...]
    unnamed x35 -> x28, local copies, waits for them, and re-layouts: 16.9 us -> 3.95 us
    reduce_sum x8 -> x1, other arithmetic: 12.1 us -> 0.14 us  [on_device(): jnp.sum(jnp.where(jnp.arange(experts_all * capacity, dtype=jnp.int32)[Non...]
    all_to_all x1 -> x0, waiting for transfers between devices: 8.46 us -> none  [on_device(): lax.all_to_all(attn, 'tp', split_axis=0, concat_axis=1, tiled=True)]
  transfers between devices with their start and end apart: 20 -> 1, of which waited for: 8 -> 1; matrix products, arithmetic and copies ran while one was open for 6% -> 0% of each run, Pallas kernels for 0% -> 0%
where the time goes in v1:
time: 194 us; the launch traced here: 193 us
  blocking collectives  71.4 us (37%)
  waiting for transfers between devices  48.6 us (25%)
  Pallas kernels  31.2 us (16%)
  matrix products  14.1 us (7%)
  other arithmetic  12.7 us (7%)
  local copies, waits for them, and re-layouts  11.5 us (6%)
  starting transfers between devices  3.79 us (2%)
    all_to_all x1, blocking collectives, on_device(): lax.all_to_all(outgoing, ('sp', 'tp'), split_axis=0, concat_axis=0, tiled...  71.4 us
    all_to_all x1, waiting for transfers between devices, on_device(): lax.all_to_all(expert_out.reshape(sources, slots, width), ('sp', 'tp'), s...  48.6 us
    pallas_call x1, Pallas kernels, attend(): pl.pallas_call(functools.partial(attention_kernel, n_sp, n_tp), out_shape...  31.2 us
    dot_general x1, matrix products, on_device(): jnp.dot(activity, down_weight[0], preferred_element_type=jnp.float32)  6.28 us
    another operation x4, other arithmetic  3.99 us
    unnamed x28, local copies, waits for them, and re-layouts  3.95 us
  transfers between devices with their start and end apart: 1, of which 1 were waited for; matrix products, arithmetic and copies ran while one was open for 0% of the time, Pallas kernels for 0%

profile of v1, /device:TPU:0, one launch (start us, length us, event | category | flops | bytes accessed | tf_op | source)
XLA Modules:
  0.0 193.5 jit_solution(4195703312387768737)
XLA Ops:
  0.0 0.9 copy.47
  0.9 0.1 eq.78
  1.1 0.7 eq.74
  1.8 0.9 fusion.24
  2.7 1.1 fusion.23
  3.8 0.8 copy.44
  4.6 0.8 copy.45
  5.4 1.3 copy.43
  6.6 0.1 multiply_reduce_fusion
  6.8 0.7 convert_element_type.70
  7.5 0.7 select_convert_fusion
  8.1 1.0 fusion.16
  9.2 0.6 add_rsqrt_fusion.1
  9.8 1.0 copy.46
  10.8 0.6 fusion.31
  11.4 1.9 reduce-window.6
  13.3 1.5 slice_reduce_fusion
  14.8 0.7 reduce-window.9
  15.6 0.9 fusion.30
  16.4 0.8 sub.25
  17.2 1.5 copy.50
  18.7 0.7 multiply_add_fusion
  19.4 0.1 convert_reduce_fusion
  19.5 0.8 multiply_multiply_fusion
  20.3 0.0 copy-done.5
  20.3 0.2 subtract_convert_fusion
  20.5 0.0 copy-start.8
  20.5 0.0 copy-start.11
  20.6 0.0 copy-start.4
  20.7 0.0 copy-start.1
  20.7 0.0 copy-start.2
  20.7 0.1 pad_maximum_fusion.q_ref
  20.8 0.7 copy-done.8
  21.4 0.1 fusion.18
  21.6 1.2 subtract_convert_fusion.2
  22.8 0.1 maximum_bitcast_fusion.1.k_ref
  22.9 31.2 %shard_map.136 = (bf16[128,2048]{1,0:T(8,128)(2,1)S(1)}, bf16[128,2048]{1,0:T(8,128)(2,1)S(1)}) custom-call(bf16[4,256,512]{2,1,0:T(8,128)(2,1)S(1)} %pad_maximum_fusion.q_ref, bf16[512,128]{1,0:T(8,128)(2,1)S(1)} %maximum_bitcast_fusion.1.k_ref, bf16[128,512]{1,0:T(8,128)(2,1)S(1)} %bitcast.55, f32[8,512]{1,0:T(8,128)S(1)} %broadcast_in_dim.23.doc_ref, ...), custom_call_target="tpu_custom_call" | custom-call | tf_op jit(solution)/shard_map/pallas_call | solution.py:212
  54.2 0.7 convolution_convert_fusion
  54.9 0.0 copy-start.12
  54.9 71.4 %all_to_all.10 = bf16[32,16,2048]{2,1,0:T(8,128)(2,1)S(1)} all-to-all(bf16[32,16,2048]{2,1,0:T(8,128)(2,1)S(1)} %bitcast.57), channel_id=1, replica_groups=mesh['sp'=8,'tp'=4] {'sp','tp'}, dimensions={0} | all-to-all | bytes 4194304 | tf_op jit(solution)/shard_map/all_to_all | solution.py:292
  126.3 1.3 copy-done.3
  127.6 2.2 %fusion.5 = f32[512,512]{1,0:T(8,128)} fusion(bf16[512,2048]{1,0:T(8,128)(2,1)S(1)} %bitcast.59, bf16[1,2048,512]{2,1,0:T(8,128)(2,1)S(1)} %copy-done.12), kind=kOutput, calls=%fused_computation.8 | convolution fusion | flops 1073741824 | bytes 5242880 | tf_op jit(solution)/shard_map/dot_general | solution.py:295
  129.8 6.3 %convolution_convert_fusion.1 = bf16[512,2048]{1,0:T(8,128)(2,1)} fusion(bf16[1,512,2048]{2,1,0:T(8,128)(2,1)S(1)} %copy-done, bf16[512,2048]{1,0:T(8,128)(2,1)} %bitcast.60, bf16[1,2048,512]{2,1,0:T(8,128)(2,1)} %param.26, f32[512,512]{1,0:T(8,128)} %fusion.5), kind=kOutput, calls=%fused_computation.1 | convolution fusion | flops 2150105088 | bytes 9437184 | tf_op jit(solution)/shard_map/dot_general | solution.py:298
  136.1 3.8 %all-to-all-start.1 = ((bf16[32,16,2048]{2,1,0:T(8,128)(2,1)}), bf16[32,16,2048]{2,1,0:T(8,128)(2,1)}, u32[]{:S(2)}, u32[]{:S(2)}) async-start(bf16[32,16,2048]{2,1,0:T(8,128)(2,1)} %bitcast.58), calls=%async_computation.1 | async-start | bytes 4194304 | tf_op jit(solution)/shard_map/all_to_all | solution.py:301
  139.9 0.1 select_reduce_fusion
  140.0 48.6 %all-to-all-done.1 = bf16[32,16,2048]{2,1,0:T(8,128)(2,1)} async-done(((bf16[32,16,2048]{2,1,0:T(8,128)(2,1)}), bf16[32,16,2048]{2,1,0:T(8,128)(2,1)}, u32[]{:S(2)}, u32[]{:S(2)}) %all-to-all-start.1) | async-done | bytes 2097184 | tf_op jit(solution)/shard_map/all_to_all | solution.py:301
  188.6 2.0 %fusion.27 = f32[128,2048]{1,0:T(8,128)S(1)} fusion(bf16[512,2048]{1,0:T(8,128)(2,1)} %bitcast.15, f32[128,512]{1,0:T(8,128)S(1)} %select_reduce_fusion), kind=kOutput, calls=%fused_computation.46 | convolution fusion | flops 268500992 | bytes 3407872 | tf_op jit(solution)/shard_map/dot_general | solution.py:320
  190.6 2.8 %fusion.1 = bf16[128,2048]{1,0:T(8,128)(2,1)} fusion(f32[128,2048]{1,0:T(8,128)S(1)} %fusion.27, bf16[512,2048]{1,0:T(8,128)(2,1)} %bitcast.15, bf16[128,2048]{1,0:T(8,128)(2,1)S(1)} %get-tuple-element.7, f32[128,512]{1,0:T(8,128)S(1)} %select_reduce_fusion), kind=kOutput, calls=%fused_computation.4 | convolution fusion | flops 269746176 | bytes 4456448 | tf_op jit(solution)/shard_map/dot_general | solution.py:320
  (25 shorter events, 0.2 us)
Async XLA Ops:
  0.0 129.8 %copy-start = (bf16[1,512,2048]{2,1,0:T(8,128)(2,1)S(1)}, bf16[1,512,2048]{2,1,0:T(8,128)(2,1)}, u32[]{:S(2)}) copy-start(bf16[1,512,2048]{2,1,0:T(8,128)(2,1)} %param.27) | copy-start | bytes 6291460
  18.7 1.6 copy-start.5
  18.7 1.7 copy-start.6
  19.5 1.1 copy-start.7
  20.5 0.9 copy-start.8
  20.5 0.9 copy-start.9
  20.5 0.9 copy-start.11
  20.6 1.0 copy-start.4
  20.7 2.3 %copy-start.1 = (bf16[128,2048]{1,0:T(8,128)(2,1)S(1)}, bf16[128,2048]{1,0:T(8,128)(2,1)}, u32[]{:S(2)}) copy-start(bf16[128,2048]{1,0:T(8,128)(2,1)} %res_ref.1) | copy-start | bytes 1572868
  20.7 2.3 %copy-start.2 = (f32[2048]{0:T(1024)S(1)}, f32[2048]{0:T(1024)}, u32[]{:S(2)}) copy-start(f32[2048]{0:T(1024)} %param.22) | copy-start | bytes 24580
  54.9 72.7 %copy-start.12 = (bf16[1,2048,512]{2,1,0:T(8,128)(2,1)S(1)}, bf16[1,2048,512]{2,1,0:T(8,128)(2,1)}, u32[]{:S(2)}) copy-start(bf16[1,2048,512]{2,1,0:T(8,128)(2,1)} %param.25) | copy-start | bytes 6291460
  126.3 1.3 copy-start.3
  136.1 3.8 %copy-start.10 = (f32[128,2]{0,1:T(2,128)S(1)}, f32[128,2]{0,1:T(2,128)}, u32[]{:S(2)}) copy-start(f32[128,2]{0,1:T(2,128)} %param.24) | copy-start | bytes 3076
  136.1 52.5 %all-to-all-start.1 = ((bf16[32,16,2048]{2,1,0:T(8,128)(2,1)}), bf16[32,16,2048]{2,1,0:T(8,128)(2,1)}, u32[]{:S(2)}, u32[]{:S(2)}) async-start(bf16[32,16,2048]{2,1,0:T(8,128)(2,1)} %bitcast.58), calls=%async_computation.1 | async-start | bytes 4194304 | tf_op jit(solution)/shard_map/all_to_all | solution.py:301

commit v2 on v1

--- a/solution.py
+++ b/solution.py
@@ -237,6 +237,142 @@
     )(q_aug, key_norm, value_t, doc_rows, residual, norm_gain.reshape(1, -1), output_weight)
 
 
+def expert_kernel(
+    n_tp, capacity, out_ref, high_ref, low_ref, hid_ref, gate_hbm, up_hbm, down_hbm,
+    new_ref,
+    gate_v, up_v, down_v, arrived, answer, returned,
+    d_send, d_recv, r_send, r_recv, w_sem,
+):
+    me = lax.axis_index("sp") * n_tp + lax.axis_index("tp")
+    devices = out_ref.shape[0] // capacity
+    rows = hid_ref.shape[0]
+    members = rows // capacity
+    groups = devices // members
+    my_group = lax.div(me, members)
+    my_place = lax.rem(me, members)
+
+    loads = [
+        pltpu.make_async_copy(source.at[0], into, w_sem.at[i])
+        for i, (source, into) in enumerate(
+            ((gate_hbm, gate_v), (up_hbm, up_v), (down_hbm, down_v))
+        )
+    ]
+    for load in loads:
+        load.start()
+
+    def place(device):
+        return (lax.div(device, n_tp), lax.rem(device, n_tp))
+
+    def slots(device):
+        return pl.ds(pl.multiple_of(device * capacity, capacity), capacity)
+
+    barrier = pltpu.get_barrier_semaphore()
+
+    def greet(i, carry):
+        there = lax.rem(me + i, devices)
+        pl.semaphore_signal(barrier, inc=1, device_id=place(there), device_id_type=MESH)
+        return carry
+
+    lax.fori_loop(1, devices, greet, 0)
+    pl.semaphore_wait(barrier, devices - 1)
+
+    def dispatch(device, landing):
+        return pltpu.make_async_remote_copy(
+            src_ref=out_ref.at[slots(device)],
+            dst_ref=arrived.at[slots(landing)],
+            send_sem=d_send.at[device],
+            recv_sem=d_recv.at[landing],
+            device_id=place(device),
+            device_id_type=MESH,
+        )
+
+    def give_back(device, landing):
+        return pltpu.make_async_remote_copy(
+            src_ref=answer.at[slots(device)],
+            dst_ref=returned.at[slots(landing)],
+            send_sem=r_send.at[device],
+            recv_sem=r_recv.at[landing],
+            device_id=place(device),
+            device_id_type=MESH,
+        )
+
+    def each(group, skip_self, act):
+        def one(i, carry):
+            act(group * members + lax.rem(my_place + i, members))
+            return carry
+
+        lax.fori_loop(1 if skip_self else 0, members, one, 0)
+
+    def group_at(step):
+        return lax.rem(my_group + step + groups, groups)
+
+    def group_rows(group):
+        return pl.ds(pl.multiple_of(group * rows, rows), rows)
+
+    for c in range(groups):
+        each(group_at(c), c == 0, lambda device: dispatch(device, me).start())
+    arrived[slots(me), :] = out_ref[slots(me), :]
+    for load in loads:
+        load.wait()
+
+    for c in range(groups):
+        group = group_at(-c)
+        each(group, c == 0, lambda device: dispatch(device, device).wait_recv())
+        x = arrived[group_rows(group), :]
+        gate_part = jnp.dot(x, gate_v[...], preferred_element_type=jnp.float32)
+        up_part = jnp.dot(x, up_v[...], preferred_element_type=jnp.float32)
+        activity = (jax.nn.silu(gate_part) * up_part).astype(jnp.bfloat16)
+        answer[group_rows(group), :] = jnp.dot(
+            activity, down_v[...], preferred_element_type=jnp.float32
+        ).astype(jnp.bfloat16)
+        each(group, c == 0, lambda device: give_back(device, me).start())
+    returned[slots(me), :] = answer[slots(me), :]
+
+    total = hid_ref[...].astype(jnp.float32)
+    for c in range(groups):
+        group = group_at(c)
+        each(group, c == 0, lambda device: give_back(device, device).wait_recv())
+        back = returned[group_rows(group), :]
+        lanes = group_rows(group)
+        total += jnp.dot(high_ref[:, lanes], back, preferred_element_type=jnp.float32)
+        total += jnp.dot(low_ref[:, lanes], back, preferred_element_type=jnp.float32)
+    new_ref[...] = total.astype(jnp.bfloat16)
+
+    for c in range(groups):
+        each(group_at(c), c == 0, lambda device: dispatch(device, me).wait_send())
+        each(group_at(c), c == 0, lambda device: give_back(device, me).wait_send())
+
+
+def run_experts(outgoing, high, low, hidden, gate_weight, up_weight, down_weight, capacity):
+    n_tp = lax.axis_size("tp")
+    devices = outgoing.shape[0] // capacity
+    vmem = pl.BlockSpec(memory_space=pltpu.VMEM)
+    anywhere = pl.BlockSpec(memory_space=pl.ANY)
+    buffer = pltpu.VMEM(outgoing.shape, jnp.bfloat16)
+    return pl.pallas_call(
+        functools.partial(expert_kernel, n_tp, capacity),
+        out_shape=jax.ShapeDtypeStruct(hidden.shape, jnp.bfloat16),
+        in_specs=[vmem] * 4 + [anywhere] * 3,
+        out_specs=vmem,
+        scratch_shapes=[
+            pltpu.VMEM(gate_weight.shape[1:], jnp.bfloat16),
+            pltpu.VMEM(up_weight.shape[1:], jnp.bfloat16),
+            pltpu.VMEM(down_weight.shape[1:], jnp.bfloat16),
+            buffer,
+            buffer,
+            buffer,
+            pltpu.SemaphoreType.DMA((devices,)),
+            pltpu.SemaphoreType.DMA((devices,)),
+            pltpu.SemaphoreType.DMA((devices,)),
+            pltpu.SemaphoreType.DMA((devices,)),
+            pltpu.SemaphoreType.DMA((3,)),
+        ],
+        compiler_params=pltpu.CompilerParams(
+            collective_id=2, has_side_effects=True, vmem_limit_bytes=40 * 1024 * 1024
+        ),
+    )(outgoing, high, low, hidden, gate_weight, up_weight, down_weight)
+
+
 def on_device(
     residual,
     query_proj,
@@ -275,10 +411,11 @@
     experts_all = lax.axis_size("sp") * lax.axis_size("tp")
     capacity = max(2, 2 * token_rows * top_count // experts_all)
     flat_ids = expert_ids.reshape(-1)
-    onehot = (flat_ids[:, None] == jnp.arange(experts_all, dtype=jnp.int32)[None, :]).astype(
-        jnp.int32
-    )
-    arrival = jnp.sum(jnp.cumsum(onehot, axis=0) * onehot, axis=1) - 1
+    order = jnp.arange(flat_ids.shape[0], dtype=jnp.int32)
+    earlier = jnp.logical_and(
+        flat_ids[:, None] == flat_ids[None, :], order[None, :] < order[:, None]
+    )
+    arrival = jnp.sum(earlier.astype(jnp.int32), axis=1)
     slot_index = flat_ids * capacity + arrival
     slot_grid = slot_index.reshape(token_rows, top_count)
     placing = jnp.sum(
@@ -288,6 +425,21 @@
         axis=2,
     ).astype(jnp.bfloat16)
     outgoing = jnp.dot(placing, normed, preferred_element_type=jnp.float32).astype(jnp.bfloat16)
+    spread = jnp.sum(
+        jnp.where(
+            jnp.arange(experts_all * capacity, dtype=jnp.int32)[None, None, :]
+            == slot_grid[:, :, None],
+            route_weights[:, :, None],
+            0.0,
+        ),
+        axis=1,
+    )
+    high = spread.astype(jnp.bfloat16)
+    low = (spread - high.astype(jnp.float32)).astype(jnp.bfloat16)
+    if capacity % 16 == 0 and token_rows % capacity == 0 and experts_all % (token_rows // capacity) == 0:
+        return run_experts(
+            outgoing, high, low, hidden, gate_weight, up_weight, down_weight, capacity
+        )
     outgoing = outgoing.reshape(experts_all, capacity, normed.shape[1])
     arrived = lax.all_to_all(outgoing, ("sp", "tp"), split_axis=0, concat_axis=0, tiled=True)
     sources, slots, width = arrived.shape
@@ -305,17 +457,6 @@
         concat_axis=0,
         tiled=True,
     )
-    spread = jnp.sum(
-        jnp.where(
-            jnp.arange(experts_all * capacity, dtype=jnp.int32)[None, None, :]
-            == slot_grid[:, :, None],
-            route_weights[:, :, None],
-            0.0,
-        ),
-        axis=1,
-    )
-    high = spread.astype(jnp.bfloat16)
-    low = (spread - high.astype(jnp.float32)).astype(jnp.bfloat16)
     rows_back = returned.reshape(experts_all * capacity, -1)
     combined = jnp.dot(high, rows_back, preferred_element_type=jnp.float32) + jnp.dot(
         low, rows_back, preferred_element_type=jnp.float32

time: 194 us -> 165 us (0.85)
  Pallas kernels: 31.2 us -> 154 us
  blocking collectives: 71.4 us -> 0 us
  waiting for transfers between devices: 48.6 us -> 0 us
  matrix products: 14.1 us -> 0.69 us
  other arithmetic: 12.7 us -> 4.03 us
  local copies, waits for them, and re-layouts: 11.5 us -> 5.71 us
  starting transfers between devices: 3.79 us -> 0 us
    pallas_call x0 -> x1, Pallas kernels: none -> 122 us  [run_experts(): pl.pallas_call(functools.partial(expert_kernel, n_tp, capacity), out_shap...]
    all_to_all x1 -> x0, blocking collectives: 71.4 us -> none  [on_device(): lax.all_to_all(outgoing, ('sp', 'tp'), split_axis=0, concat_axis=0, tiled...]
    all_to_all x1 -> x0, waiting for transfers between devices: 48.6 us -> none  [on_device(): lax.all_to_all(expert_out.reshape(sources, slots, width), ('sp', 'tp'), s...]
    dot_general x4 -> x0, matrix products: 13.4 us -> none  [the longest x1 6.28 us: on_device(): jnp.dot(activity, down_weight[0], preferred_element_type=jnp.float32)]
    all_to_all x1 -> x0, starting transfers between devices: 3.79 us -> none  [on_device(): lax.all_to_all(expert_out.reshape(sources, slots, width), ('sp', 'tp'), s...]
    another operation x4 -> x2, other arithmetic: 3.99 us -> 1.38 us
    sub x2 -> x0, local copies, waits for them, and re-layouts: 2.26 us -> none  [on_device(): arrival = jnp.sum(jnp.cumsum(onehot, axis=0) * onehot, axis=1) - 1]
    unnamed x28 -> x29, local copies, waits for them, and re-layouts: 3.95 us -> 4.89 us
  transfers between devices with their start and end apart: 1 -> 0, of which waited for: 1 -> 0; matrix products, arithmetic and copies ran while one was open for 0% -> 0% of each run, Pallas kernels for 0% -> 0%
where the time goes in v2:
time: 165 us; the launch traced here: 164 us
  Pallas kernels  154 us (93%)
  local copies, waits for them, and re-layouts  5.71 us (3%)
  other arithmetic  4.03 us (2%)
    pallas_call x1, Pallas kernels, run_experts(): pl.pallas_call(functools.partial(expert_kernel, n_tp, capacity), out_shap...  122 us
    pallas_call x1, Pallas kernels, attend(): pl.pallas_call(functools.partial(attention_kernel, n_sp, n_tp), out_shape...  31.2 us
    unnamed x29, local copies, waits for them, and re-layouts  4.89 us

profile of v2, /device:TPU:0, one launch (start us, length us, event | category | flops | bytes accessed | tf_op | source)
XLA Modules:
  0.0 164.3 jit_solution(6326406131868241553)
XLA Ops:
  0.0 0.2 fusion.9
  0.2 0.0 copy-start.11
  0.2 1.1 fusion.8
  1.4 0.1 copy.42
  1.5 0.1 copy.43
  1.6 0.0 copy-done.5
  1.6 0.2 copy.41
  1.8 0.1 multiply_reduce_fusion
  2.0 0.0 copy-done.11
  2.0 0.0 copy-start.9
  2.0 0.2 multiply_multiply_fusion
  2.2 0.2 subtract_convert_fusion
  2.4 0.0 copy-start.6
  2.4 0.0 copy-start.12
  2.5 0.2 copy-done.9
  2.8 0.0 copy-start.7
  2.8 0.0 copy-start.3
  2.8 0.0 copy-start.4
  2.8 0.1 pad_maximum_fusion.q_ref
  2.9 0.4 copy-done.6
  3.3 0.1 fusion
  3.5 0.0 copy-done.12
  3.5 0.1 fusion.2
  3.6 1.2 subtract_convert_fusion.2
  4.8 0.1 maximum_bitcast_fusion.1.k_ref
  4.9 0.0 copy-done.7
  5.0 0.1 copy.44
  5.1 0.0 copy-done.3
  5.1 0.0 copy-done.4
  5.1 0.0 copy-start.8
  5.1 31.2 %shard_map.136 = (bf16[128,2048]{1,0:T(8,128)(2,1)S(1)}, bf16[128,2048]{1,0:T(8,128)(2,1)S(1)}) custom-call(bf16[4,256,512]{2,1,0:T(8,128)(2,1)S(1)} %pad_maximum_fusion.q_ref, bf16[512,128]{1,0:T(8,128)(2,1)S(1)} %maximum_bitcast_fusion.1.k_ref, bf16[128,512]{1,0:T(8,128)(2,1)S(1)} %bitcast.17, f32[8,512]{1,0:T(8,128)S(1)} %broadcast_in_dim.23.doc_ref, ...), custom_call_target="tpu_custom_call" | custom-call | tf_op jit(solution)/shard_map/pallas_call | solution.py:212
  36.4 0.0 copy-start.10
  36.4 0.0 copy-start
  36.4 0.0 copy-done.8
  36.4 0.1 copy.39
  36.5 0.1 eq.61
  36.6 0.2 convert_reduce_fusion.1
  36.8 0.1 reduce_sum.48
  37.0 0.1 copy.40
  37.0 0.1 convert_reduce_fusion
  37.1 0.7 convolution_convert_fusion.out_ref
  37.8 0.0 copy-done.10
  37.9 0.1 select_reduce_fusion
  38.0 0.0 copy-start.1
  38.1 1.6 copy-done.1
  39.6 1.6 copy-done.2
  41.2 122.3 %shard_map.137 = bf16[128,2048]{1,0:T(8,128)(2,1)S(1)} custom-call(bf16[512,2048]{1,0:T(8,128)(2,1)S(1)} %convolution_convert_fusion.out_ref, bf16[128,512]{1,0:T(8,128)(2,1)S(1)} %get-tuple-element.10.high_ref, bf16[128,512]{1,0:T(8,128)(2,1)S(1)} %get-tuple-element.9.low_ref, bf16[128,2048]{1,0:T(8,128)(2,1)S(1)} %get-tuple-element.8.hid_ref, ...), custom_call_target="tpu_custom_call" | custom-call | tf_op jit(solution)/shard_map/pallas_call | solution.py:352
  163.6 0.8 copy.46
  (14 shorter events, 0.2 us)
Async XLA Ops:
  0.0 1.6 copy-start.5
  0.2 1.8 %copy-start.11 = (f32[128]{0:T(128)S(1)}, f32[128]{0:T(128)}, u32[]{:S(2)}) copy-start(f32[128]{0:T(128)} %param.18) | copy-start | bytes 1540
  2.0 0.7 copy-start.9
  2.4 0.9 copy-start.6
  2.4 1.1 copy-start.12
  2.8 2.2 %copy-start.7 = (bf16[512,128]{1,0:T(8,128)(2,1)S(1)}, bf16[512,128]{1,0:T(8,128)(2,1)}, u32[]{:S(2)}) copy-start(bf16[512,128]{1,0:T(8,128)(2,1)} %param.17) | copy-start | bytes 393220
  2.8 2.3 %copy-start.3 = (bf16[128,2048]{1,0:T(8,128)(2,1)S(1)}, bf16[128,2048]{1,0:T(8,128)(2,1)}, u32[]{:S(2)}) copy-start(bf16[128,2048]{1,0:T(8,128)(2,1)} %res_ref.1) | copy-start | bytes 1572868
  2.8 2.3 %copy-start.4 = (f32[2048]{0:T(1024)S(1)}, f32[2048]{0:T(1024)}, u32[]{:S(2)}) copy-start(f32[2048]{0:T(1024)} %param.22) | copy-start | bytes 24580
  5.1 31.3 %copy-start.8 = (s32[128,2]{0,1:T(2,128)S(1)}, s32[128,2]{0,1:T(2,128)}, u32[]{:S(2)}) copy-start(s32[128,2]{0,1:T(2,128)} %param.23) | copy-start | bytes 3076
  36.4 1.5 copy-start.10
  36.4 1.7 %copy-start = (bf16[1,2048,512]{2,1,0:T(8,128)(2,1)S(1)}, bf16[1,2048,512]{2,1,0:T(8,128)(2,1)}, u32[]{:S(2)}) copy-start(bf16[1,2048,512]{2,1,0:T(8,128)(2,1)} %gate_hbm.1) | copy-start | bytes 6291460
  38.0 1.6 copy-start.1
  39.6 1.6 copy-start.2
